TPU v7x, 32 devices: a whole 2x2x4 slice. The times are simulated.
32 devices in a mesh: sp: 16 (over z, y, x), tp: 2 (over core).
Axes of the slice: x: 2, y: 2, z: 4, core: 2. Of those that a mesh axis runs over, the one named last changes fastest.
Arguments:
- tokens: bfloat16 [6144, 2048], P('sp', 'tp'), may hold values from -1620 to 1620
- input_norm_gain: float32 [2048], replicated, may hold values from 0.1 to 1.9
- outer_gate_weight: bfloat16 [2048, 1024], P(None, 'tp'), may hold values from -0.125 to 0.125
- inner_gate_weight: bfloat16 [2048, 1024], P(None, 'tp'), may hold values from -0.125 to 0.125
- convolution_input_weight: bfloat16 [2048, 1024], P(None, 'tp'), may hold values from -0.125 to 0.125
- convolution_kernel_taps: bfloat16 [3, 1024], P(None, 'tp'), may hold values from -3 to 3
- query_weight_matrix: bfloat16 [2048, 512], P(None, 'tp'), may hold values from -0.125 to 0.125
- key_weight_matrix: bfloat16 [2048, 512], P(None, 'tp'), may hold values from -0.125 to 0.125
- value_weight_matrix: bfloat16 [2048, 1024], P(None, 'tp'), may hold values from -0.125 to 0.125
- forget_gate_weight: bfloat16 [2048, 512], P(None, 'tp'), may hold values from -0.125 to 0.125
- attention_gate_weight: bfloat16 [2048, 1024], P(None, 'tp'), may hold values from -0.125 to 0.125
- forget_gate_bias: float32 [512], P('tp'), may hold values from -1.5 to 10
- extra_logarithm_decay: float32 [6144, 16], P('sp', 'tp'), may hold values from -0.72 to 0
- initial_head_state: float32 [16, 32, 64], P('tp'), may hold values from -768 to 768
- head_norm_gain: float32 [64], replicated, may hold values from 0.1 to 1.9
- convolution_output_weight: bfloat16 [1024, 2048], P('tp'), may hold values from -0.125 to 0.125
- attention_output_weight: bfloat16 [1024, 2048], P('tp'), may hold values from -0.125 to 0.125
Outputs:
- mixed: bfloat16 [6144, 2048], P(('sp', 'tp'))
All inputs are finite; a program needn't handle non-finite values.
Results may differ from a plain program's by a relative error of at most 0.017.
Values may be sent and summed in bfloat16 or wider, within the bound.
A program may use at most 128 MiB of HBM per device.

v0:
```python
import jax
import jax.numpy as jnp
from jax import lax
from jax.sharding import PartitionSpec as P

BLOCK = 64


NORM_EPS = 1e-06
GATE_SOFTNESS = 16.0


def from_behind(block, axis, distance):
    devices = range(lax.axis_size(axis))
    route = [(i - distance, i) for i in devices if i - distance in devices]
    return lax.ppermute(block, axis, route)


def prefix(part, axis, combine, identity):
    place = lax.axis_index(axis)
    gathered = jax.tree.map(lambda a: lax.all_gather(a, axis), part)
    state = jax.tree.map(lambda a, e: jnp.zeros_like(a) + jnp.asarray(e, a.dtype), part, identity)

    def one(turn, state):
        return combine(
            state, jax.tree.map(lambda a: lax.dynamic_index_in_dim(a, turn, 0, False), gathered)
        )

    return lax.fori_loop(0, place, one, state)


def block_terms(queries, key_rows, values, logarithm_decay):
    cumulative = jnp.cumsum(logarithm_decay, axis=1)
    last_log = cumulative[:, -1:]
    query_g = queries * jnp.exp(cumulative)
    key_g = key_rows * jnp.exp(-cumulative)
    scores = jnp.einsum("nihd,njhd->nhij", query_g, key_g, precision=lax.Precision.HIGHEST)
    width = queries.shape[1]
    causal = jnp.arange(width)[:, None] >= jnp.arange(width)[None, :]
    scores = jnp.where(causal, scores, 0.0)
    inner = jnp.einsum("nhij,njhe->nihe", scores, values, precision=lax.Precision.HIGHEST)
    key_decayed = key_rows * jnp.exp(last_log - cumulative)
    update = jnp.einsum("nchd,nche->nhde", key_decayed, values, precision=lax.Precision.HIGHEST)
    return (query_g, inner, update, last_log[:, 0])


def carry_step(state, inputs):
    block_decay, update = inputs
    return (block_decay[..., None] * state + update, state)


def chain_join(earlier, later):
    return (earlier[0] * later[0], later[0][..., None] * earlier[1] + later[1])


def on_device(
    tokens,
    input_norm_gain,
    outer_gate_weight,
    inner_gate_weight,
    convolution_input_weight,
    convolution_kernel_taps,
    query_weight_matrix,
    key_weight_matrix,
    value_weight_matrix,
    forget_gate_weight,
    attention_gate_weight,
    forget_gate_bias,
    extra_logarithm_decay,
    initial_head_state,
    head_norm_gain,
    convolution_output_weight,
    attention_output_weight,
):
    number_of_rows = tokens.shape[0]
    number_of_heads, key_channel_count, value_dim = initial_head_state.shape
    weights = (
        outer_gate_weight,
        inner_gate_weight,
        convolution_input_weight,
        query_weight_matrix,
        key_weight_matrix,
        value_weight_matrix,
        forget_gate_weight,
        attention_gate_weight,
    )
    whole_rows = lax.all_gather(tokens, "tp", axis=1, tiled=True).astype(jnp.float32)
    power = jnp.mean(whole_rows * whole_rows, axis=1, keepdims=True)
    normed = (whole_rows * lax.rsqrt(power + NORM_EPS) * input_norm_gain).astype(jnp.bfloat16)
    sums = tuple(
        (jnp.dot(normed, weight, preferred_element_type=jnp.float32) for weight in weights)
    )
    conv_b, conv_c, conv_h, query, key_proj, value, forget_preactivation, out_gate = (
        term.astype(jnp.bfloat16) for term in sums
    )
    product = (conv_c.astype(jnp.float32) * conv_h.astype(jnp.float32)).astype(jnp.bfloat16)
    tap_count = convolution_kernel_taps.shape[0]
    previous = from_behind(product[number_of_rows - tap_count + 1 :], "sp", 1)
    padded = jnp.concatenate([previous, product], axis=0)
    conv = jnp.zeros(product.shape, jnp.float32)
    for tap_index in range(tap_count):
        conv = conv + convolution_kernel_taps[tap_index].astype(jnp.float32) * padded[
            tap_index : tap_index + number_of_rows
        ].astype(jnp.float32)
    conv_out = (conv_b.astype(jnp.float32) * conv).astype(jnp.bfloat16)
    logarithm_decay = (
        jax.nn.log_sigmoid(forget_preactivation.astype(jnp.float32) + forget_gate_bias)
        / GATE_SOFTNESS
    )
    logarithm_decay = (
        logarithm_decay.reshape(number_of_rows, number_of_heads, key_channel_count)
        + extra_logarithm_decay[:, :, None]
    )
    n_blocks = number_of_rows // BLOCK
    queries = (query.astype(jnp.float32) * key_channel_count ** (-0.5)).reshape(
        n_blocks, BLOCK, number_of_heads, key_channel_count
    )
    key_rows = key_proj.astype(jnp.float32).reshape(
        n_blocks, BLOCK, number_of_heads, key_channel_count
    )
    values = value.astype(jnp.float32).reshape(n_blocks, BLOCK, number_of_heads, value_dim)
    query_g, inner, update, block_log = block_terms(
        queries,
        key_rows,
        values,
        logarithm_decay.reshape(n_blocks, BLOCK, number_of_heads, key_channel_count),
    )
    zero_state = jnp.zeros((number_of_heads, key_channel_count, value_dim), jnp.float32)
    local_final, entering = lax.scan(carry_step, zero_state, (jnp.exp(block_log), update))
    exclusive = jnp.cumsum(block_log, axis=0) - block_log
    device_decay = jnp.exp(jnp.sum(block_log, axis=0))
    prefix_decay, prefix_state = prefix(
        (device_decay, local_final), "sp", chain_join, (jnp.ones_like(device_decay), zero_state)
    )
    incoming = prefix_state + prefix_decay[..., None] * initial_head_state
    entering = entering + jnp.exp(exclusive)[..., None] * incoming[None]
    outer = jnp.einsum("nchd,nhde->nche", query_g, entering, precision=lax.Precision.HIGHEST)
    raw = (inner + outer).reshape(number_of_rows, number_of_heads, value_dim)
    raw = raw * lax.rsqrt(jnp.mean(raw * raw, axis=2, keepdims=True) + NORM_EPS) * head_norm_gain
    gate_values = jax.nn.silu(out_gate.astype(jnp.float32)).reshape(
        number_of_rows, number_of_heads, value_dim
    )
    attn_out = (
        (raw * gate_values)
        .reshape(number_of_rows, number_of_heads * value_dim)
        .astype(jnp.bfloat16)
    )
    return lax.psum_scatter(
        (
            jnp.dot(conv_out, convolution_output_weight, preferred_element_type=jnp.float32)
            + jnp.dot(attn_out, attention_output_weight, preferred_element_type=jnp.float32)
        ).astype(jnp.bfloat16),
        "tp",
        scatter_dimension=0,
        tiled=True,
    )


def solution(mesh):
    placed = (
        P("sp", "tp"),
        P(),
        P(None, "tp"),
        P(None, "tp"),
        P(None, "tp"),
        P(None, "tp"),
        P(None, "tp"),
        P(None, "tp"),
        P(None, "tp"),
        P(None, "tp"),
        P(None, "tp"),
        P("tp"),
        P("sp", "tp"),
        P("tp", None, None),
        P(),
        P("tp", None),
        P("tp", None),
    )
    return jax.shard_map(
        on_device, mesh=mesh, in_specs=placed, out_specs=P(("sp", "tp"), None), check_vma=False
    )
```

profile of v0, /device:TPU:0, one launch (start us, length us, event | category | flops | bytes accessed | tf_op | source)
XLA Modules:
  0.0 176.2 jit_solution(7418654759086508791)
XLA Ops:
  6.5 0.7 all-gather.5.cloned.1.call-update
  7.3 0.7 mul.190
  8.1 0.8 add.99
  8.9 0.8 slice_convert_fusion.2
  9.7 11.8 %all-gather.5.cloned.1.call-done = bf16[384,2048]{1,0:T(8,128)(2,1)} async-done(((bf16[384,1024]{1,0:T(8,128)(2,1)}), bf16[384,2048]{1,0:T(8,128)(2,1)}) %all-gather.5.cloned.1.call-update) | async-done | bytes 1572880 | tf_op jit(solution)/shard_map/all_gather | solution.py:87
  21.4 1.9 %fusion = f32[384]{0:T(512)S(1)} fusion(bf16[384,2048]{1,0:T(8,128)(2,1)} %all-gather.5.cloned.1.call-done), kind=kLoop, calls=%fused_computation.7 | loop fusion | flops 2358912 | bytes 1574400 | tf_op jit(solution)/shard_map/reduce_sum | solution.py:88
  23.4 2.0 %fusion.42 = f32[384,256]{1,0:T(8,128)S(1)} fusion(bf16[2048,256]{1,0:T(8,128)(2,1)} %param.30, f32[256]{0:T(256)S(1)} %copy-done.13, bf16[384,2048]{1,0:T(8,128)(2,1)S(1)} %copy-done.5, f32[2048]{0:T(1024)S(1)} %copy-done.12, f32[384]{0:T(512)S(1)} %add_rsqrt_fusion.1), kind=kOutput, calls=%fused_computation.68 | convolution fusion | flops 406978560 | bytes 3025408 | tf_op jit(solution)/shard_map/dot_general | solution.py:91
  25.4 0.9 copy.52
  26.4 1.2 reshape.85
  27.6 1.1 broadcast_add_fusion
  28.6 2.9 %copy.53 = f32[6,64,8,32]{3,2,1,0:T(8,128)} copy(f32[6,64,8,32]{1,0,3,2:T(8,128)} %broadcast_add_fusion) | data formatting | bytes 786432 | tf_op jit(solution)/shard_map/add | solution.py:111
  31.5 1.6 fusion.66
  33.2 1.1 copy-done.4
  34.3 2.6 %convolution_convert_fusion.1 = bf16[384,512]{1,0:T(8,128)(2,1)S(1)} fusion(bf16[2048,512]{1,0:T(8,128)(2,1)} %param.29, bf16[384,2048]{1,0:T(8,128)(2,1)S(1)} %copy-done.6, f32[2048]{0:T(1024)S(1)} %copy-done.12, f32[384]{0:T(512)S(1)} %add_rsqrt_fusion.1), kind=kOutput, calls=%fused_computation.24 | convolution fusion | flops 808648704 | bytes 4072960 | tf_op jit(solution)/shard_map/dot_general | solution.py:91
  37.4 2.6 %fusion.17 = f32[384,256]{1,0:T(8,128)S(1)} fusion(bf16[2048,256]{1,0:T(8,128)(2,1)} %param.28, bf16[384,2048]{1,0:T(8,128)(2,1)} %all-gather.5.cloned.1.call-done, f32[2048]{0:T(1024)S(1)} %copy-done.12, f32[384]{0:T(512)S(1)} %add_rsqrt_fusion.1), kind=kOutput, calls=%fused_computation.37 | convolution fusion | flops 405995520 | bytes 3024384 | tf_op jit(solution)/shard_map/dot_general | solution.py:91
  40.0 1.5 reshape.97
  41.5 2.3 %fusion.22 = f32[384,256]{1,0:T(8,128)S(1)} fusion(bf16[2048,256]{1,0:T(8,128)(2,1)} %param.27, bf16[384,2048]{1,0:T(8,128)(2,1)} %all-gather.5.cloned.1.call-done, f32[2048]{0:T(1024)S(1)} %copy-done.12, f32[384]{0:T(512)S(1)} %add_rsqrt_fusion.1), kind=kOutput, calls=%fused_computation.44 | convolution fusion | flops 406093824 | bytes 3024384 | tf_op jit(solution)/shard_map/dot_general | solution.py:91
  43.9 1.5 reshape.96
  45.4 4.6 %exponential_multiply_fusion = (f32[6,64,8,32]{3,2,1,0:T(8,128)S(1)}, f32[6,64,8,32]{3,2,1,0:T(8,128)}, f32[6,64,8,32]{3,2,1,0:T(8,128)}) fusion(f32[6,64,8,32]{3,2,1,0:T(8,128)} %reshape.97, f32[6,64,8,32]{3,2,1,0:T(8,128)} %copy-done.4, f32[6,8,32]{2,1,0:T(8,128)S(1)} %get-tuple-element.116, f32[6,64,8,32]{3,2,1,0:T(8,128)} %reshape.96), kind=kLoop, calls=%fused_computation.17 | loop fusion | flops 491520 | bytes 2365440 | tf_op jit(solution)/shard_map/mul | solution.py:42
  50.0 2.3 %fusion.3 = f32[6,8,32,64]{3,2,1,0:T(8,128)} fusion(f32[6,64,8,32]{3,2,1,0:T(8,128)S(1)} %get-tuple-element.113, bf16[6,64,8,64]{3,2,1,0:T(8,128)(2,1)S(1)} %reshape.83), kind=kOutput, calls=%fused_computation.11 | convolution fusion | flops 75497472 | bytes 1179648 | tf_op jit(solution)/shard_map/nchd,nche->nhde/dot_general | solution.py:43
  52.3 10.3 %while.26 = (s32[]{:T(128)}, f32[8,32,64]{2,1,0:T(8,128)S(1)}, f32[6,8,32,64]{3,2,1,0:T(8,128)}, f32[6,8,32]{2,1,0:T(8,128)S(1)}, f32[6,8,32,64]{3,2,1,0:T(8,128)}, /*index=5*/s32[]{:T(128)}, s32[]{:T(128)}) while((s32[]{:T(128)}, f32[8,32,64]{2,1,0:T(8,128)S(1)}, f32[6,8,32,64]{3,2,1,0:T(8,128)}, f32[6,8,32]{2,1,0:T(8,128)S(1)}, ...), condition=%wide.region_3.4_spmd.clone, body=%wide.region_2.3_spmd.clone.sunk | while | flops 65539 | bytes 396396 | solution.py:129
  52.3 0.7 bitcast_dynamic-update-slice_fusion.2
  53.0 1.0 bitcast_add_fusion.5
  54.0 0.7 bitcast_dynamic-update-slice_fusion.2
  54.7 1.0 bitcast_add_fusion.5
  55.8 0.7 bitcast_dynamic-update-slice_fusion.2
  56.4 1.0 bitcast_add_fusion.5
  57.5 0.7 bitcast_dynamic-update-slice_fusion.2
  58.2 1.0 bitcast_add_fusion.5
  59.2 0.7 bitcast_dynamic-update-slice_fusion.2
  59.9 1.0 bitcast_add_fusion.5
  61.0 0.7 bitcast_dynamic-update-slice_fusion.2
  61.6 1.0 bitcast_add_fusion.5
  63.4 3.2 %fusion.13 = f32[384,512]{1,0:T(8,128)S(1)} fusion(bf16[2048,512]{1,0:T(8,128)(2,1)} %param.24, bf16[384,2048]{1,0:T(8,128)(2,1)} %all-gather.5.cloned.1.call-done, f32[2048]{0:T(1024)S(1)} %copy-done.12, f32[384]{0:T(512)S(1)} %add_rsqrt_fusion.1), kind=kOutput, calls=%fused_computation.30 | convolution fusion | flops 808845312 | bytes 4466176 | tf_op jit(solution)/shard_map/dot_general | solution.py:91
  66.7 1.0 fusion.12
  67.7 3.8 %collective-permute-start = (bf16[2,512]{1,0:T(2,128)(2,1)S(1)}, bf16[2,512]{1,0:T(2,128)(2,1)S(1)}, u32[]{:S(2)}, u32[]{:S(2)}) collective-permute-start(bf16[2,512]{1,0:T(2,128)(2,1)S(1)} %slice.28), channel_id=1, source_target_pairs={{0,2},{2,4},{4,6},{6,8},{8,10},{10,12},{12,14},{14,16},{16,18},{18... | collective-permute-start | bytes 6152 | tf_op jit(solution)/shard_map/ppermute | solution.py:16
  71.6 1.9 %copy.57 = f32[6,64,8,32]{1,3,2,0:T(8,128)S(1)} copy(f32[6,64,8,32]{3,2,1,0:T(8,128)} %get-tuple-element.117) | data formatting | bytes 786432 | tf_op jit(solution)/shard_map/mul | solution.py:35
  73.5 1.0 fusion.23
  74.5 4.4 %fusion.5 = f32[6,8,64,64]{3,2,1,0:T(8,128)S(1)} fusion(f32[6,64,8,32]{1,3,2,0:T(8,128)S(1)} %copy.57, f32[6,64,8,32]{3,2,1,0:T(8,128)} %get-tuple-element.114), kind=kOutput, calls=%fused_computation.13 | convolution fusion | flops 75497472 | bytes 1572864 | tf_op jit(solution)/shard_map/nihd,njhd->nhij/dot_general | solution.py:37
  78.8 2.7 %fusion.7 = f32[6,8,64,64]{3,2,1,0:T(8,128)} fusion(f32[6,8,64,64]{3,2,1,0:T(8,128)S(1)} %fusion.5, pred[64,64]{1,0:T(8,128)(4,1)S(1)} %iota_compare_fusion, bf16[6,64,8,64]{3,2,1,0:T(8,128)(2,1)S(1)} %copy-done.3), kind=kOutput, calls=%fused_computation.18 | convolution fusion | flops 151191552 | bytes 1970176 | tf_op jit(solution)/shard_map/nhij,njhe->nihe/dot_general | solution.py:41
  81.5 39.2 %all-gather = f32[128,32]{1,0:T(8,128)S(1)} all-gather(f32[8,32]{1,0:T(8,128)S(1)} %exp.47), channel_id=2, replica_groups=mesh['sp'=16,'tp'=2] {'sp'}, dimensions={0}, use_global_device_ids=true | all-gather | bytes 17408 | tf_op jit(solution)/shard_map/all_gather | solution.py:21
  120.7 6.1 %fusion.24 = f32[384,2048]{1,0:T(8,128)} fusion(bf16[512,2048]{1,0:T(8,128)(2,1)S(1)} %copy-done, bf16[2048,512]{1,0:T(8,128)(2,1)} %param.23, bf16[384,512]{1,0:T(8,128)(2,1)} %copy-done.10, bf16[2,512]{1,0:T(2,128)(2,1)S(1)} %collective-permute-done, f32[512]{0:T(512)S(1)} %bitcast.57, f32[512]{0:T(512)S(1)} %bitcast.58, f32[512]{0:T(512)S(1)} %bitcast.56, ...), kind=kOutput, calls=%fused_computation.47 | convolution fusion | flops 1617297408 | bytes 9324032 | tf_op jit(solution)/shard_map/dot_general | solution.py:150
  127.8 5.7 %multiply_reduce_fusion = (f32[6,64,8]{1,2,0:T(8,128)S(1)}, f32[6,64,8,64]{1,3,2,0:T(8,128)}) fusion(f32[6,8,64,64]{3,2,1,0:T(8,128)} %fusion.7, f32[6,64,8,32]{1,3,2,0:T(8,128)S(1)} %copy.57, f32[6,8,32,64]{3,2,1,0:T(8,128)} %get-tuple-element.67, f32[8,32,64]{2,1,0:T(8,128)S(1)} %multiply_add_fusion, f32[6,8,32]{2,1,0:T(8,128)S(1)} %fusion.23), kind=kOutput, calls=%fused_computation.15 | convolution fusion | flops 76280832 | bytes 2443264 | tf_op jit(solution)/shard_map/nchd,nhde->nche/dot_general | solution.py:137
  133.7 1.2 copy.66
  134.9 3.0 %copy.64 = f32[6,64,8,64]{3,2,1,0:T(8,128)} copy(f32[6,64,8,64]{1,3,2,0:T(8,128)} %get-tuple-element.122) | data formatting | bytes 1572864 | tf_op jit(solution)/shard_map/add | solution.py:138
  137.9 2.6 %reshape.88 = f32[384,512]{1,0:T(8,128)} reshape(f32[6,64,8,64]{3,2,1,0:T(8,128)} %copy.64) | data formatting | bytes 1572864 | tf_op jit(solution)/shard_map/reshape | solution.py:138
  140.6 7.0 %add_convert_fusion = bf16[384,2048]{1,0:T(8,128)(2,1)} fusion(f32[384,2048]{1,0:T(8,128)} %fusion.24, bf16[512,2048]{1,0:T(8,128)(2,1)} %param.37, bf16[2048,512]{1,0:T(8,128)(2,1)} %param.31, f32[384,512]{1,0:T(8,128)} %reshape.88, f32[384,512]{1,0:T(8,128)S(1)} %copy-done.8, f32[512]{0:T(512)S(1)} %mul.191, ...), kind=kOutput, calls=%fused_computation.10 | convolution fusion | flops 1617297408 | bytes 12070400 | tf_op jit(solution)/shard_map/dot_general | solution.py:151
  147.6 22.0 %reduce-scatter.2.cloned.1.call-done = bf16[192,2048]{1,0:T(8,128)(2,1)} async-done(((bf16[384,2048]{1,0:T(8,128)(2,1)}), bf16[192,2048]{1,0:T(8,128)(2,1)}) %reduce-scatter.2.cloned.1.call-update) | async-done | bytes 786448 | tf_op jit(solution)/shard_map/reduce_scatter | solution.py:148
  (58 shorter events, 2.5 us)
Async XLA Ops:
  6.5 114.1 %copy-start = (bf16[512,2048]{1,0:T(8,128)(2,1)S(1)}, bf16[512,2048]{1,0:T(8,128)(2,1)}, u32[]{:S(2)}) copy-start(bf16[512,2048]{1,0:T(8,128)(2,1)} %param.36) | copy-start | bytes 6291460
  6.5 16.8 %copy-start.12 = (f32[2048]{0:T(1024)S(1)}, f32[2048]{0:T(1024)}, u32[]{:S(2)}) copy-start(f32[2048]{0:T(1024)} %param.22) | copy-start | bytes 24580
  6.5 16.8 %copy-start.13 = (f32[256]{0:T(256)S(1)}, f32[256]{0:T(256)}, u32[]{:S(2)}) copy-start(f32[256]{0:T(256)} %param.32) | copy-start | bytes 3076
  6.5 14.9 %all-gather.5.cloned.1.call-start = ((), (), s32[]{:S(2)}) async-start(), calls=%async_computation.1 | async-start | bytes 2359296 | tf_op jit(solution)/shard_map/all_gather | solution.py:87
  7.3 119.5 %all-gather.7.cloned.1.call-start = ((), (), s32[]{:S(2)}) async-start(), calls=%async_computation.3 | async-start | bytes 2228224 | tf_op jit(solution)/shard_map/all_gather | solution.py:21
  21.4 1.9 %copy-start.5 = (bf16[384,2048]{1,0:T(8,128)(2,1)S(1)}, bf16[384,2048]{1,0:T(8,128)(2,1)}, u32[]{:S(2)}) copy-start(bf16[384,2048]{1,0:T(8,128)(2,1)} %all-gather.5.cloned.1.call-done) | copy-start | bytes 4718596
  31.5 2.8 %copy-start.6 = (bf16[384,2048]{1,0:T(8,128)(2,1)S(1)}, bf16[384,2048]{1,0:T(8,128)(2,1)}, u32[]{:S(2)}) copy-start(bf16[384,2048]{1,0:T(8,128)(2,1)} %all-gather.5.cloned.1.call-done) | copy-start | bytes 4718596
  33.2 1.2 copy-start.4
  37.3 12.6 %copy-start.2 = (bf16[6,64,8,64]{3,2,1,0:T(8,128)(2,1)}, bf16[6,64,8,64]{3,2,1,0:T(8,128)(2,1)S(1)}, u32[]{:S(2)}) copy-start(bf16[6,64,8,64]{3,2,1,0:T(8,128)(2,1)S(1)} %reshape.83) | copy-start | bytes 1179652
  62.7 0.7 copy-start.1
  63.3 106.3 %reduce-scatter.2.cloned.1.call-start = ((), (), s32[]{:S(2)}) async-start(), calls=%async_computation.2 | async-start | bytes 2359296 | tf_op jit(solution)/shard_map/reduce_scatter | solution.py:148
  63.4 3.3 %copy-start.7 = (bf16[384,2048]{1,0:T(8,128)(2,1)S(1)}, bf16[384,2048]{1,0:T(8,128)(2,1)}, u32[]{:S(2)}) copy-start(bf16[384,2048]{1,0:T(8,128)(2,1)} %all-gather.5.cloned.1.call-done) | copy-start | bytes 4718596
  63.4 3.3 %copy-start.11 = (bf16[2048,512]{1,0:T(8,128)(2,1)S(1)}, bf16[2048,512]{1,0:T(8,128)(2,1)}, u32[]{:S(2)}) copy-start(bf16[2048,512]{1,0:T(8,128)(2,1)} %param.25) | copy-start | bytes 6291460
  67.7 3.8 %copy-start.10 = (bf16[384,512]{1,0:T(8,128)(2,1)}, bf16[384,512]{1,0:T(8,128)(2,1)S(1)}, u32[]{:S(2)}) copy-start(bf16[384,512]{1,0:T(8,128)(2,1)S(1)} %fusion.12) | copy-start | bytes 1179652
  67.7 52.9 %collective-permute-start = (bf16[2,512]{1,0:T(2,128)(2,1)S(1)}, bf16[2,512]{1,0:T(2,128)(2,1)S(1)}, u32[]{:S(2)}, u32[]{:S(2)}) collective-permute-start(bf16[2,512]{1,0:T(2,128)(2,1)S(1)} %slice.28), channel_id=1, source_target_pairs={{0,2},{2,4},{4,6},{6,8},{8,10},{10,12},{12,14},{14,16},{16,18},{18... | collective-permute-start | bytes 6152 | tf_op jit(solution)/shard_map/ppermute | solution.py:16
  74.5 4.4 %copy-start.3 = (bf16[6,64,8,64]{3,2,1,0:T(8,128)(2,1)S(1)}, bf16[6,64,8,64]{3,2,1,0:T(8,128)(2,1)}, u32[]{:S(2)}) copy-start(bf16[6,64,8,64]{3,2,1,0:T(8,128)(2,1)} %copy-done.2) | copy-start | bytes 1179652
  126.8 0.9 copy-start.9
  137.9 2.6 %copy-start.8 = (f32[384,512]{1,0:T(8,128)S(1)}, f32[384,512]{1,0:T(8,128)}, u32[]{:S(2)}) copy-start(f32[384,512]{1,0:T(8,128)} %copy.66) | copy-start | bytes 2359300
Sparse Core Ops, SparseCore 0:
  8.9 12.5 all-gather.4
  63.5 61.8 all-gather.6
  147.7 21.8 reduce-scatter.1
where the time goes:
time: 177 us; the launch traced here: 176 us
  matrix products  42 us (24%)
  blocking collectives  39.2 us (22%)
  waiting for transfers between devices  34.5 us (19%)
  local copies, waits for them, and re-layouts  21.5 us (12%)
  other arithmetic  21.3 us (12%)
  between operations  13.4 us (8%)
  starting transfers between devices  3.88 us (2%)
    all_gather x1, blocking collectives, prefix(): gathered = jax.tree.map(lambda a: lax.all_gather(a, axis), part)  39.2 us
    reduce_scatter x1, waiting for transfers between devices, on_device(): lax.psum_scatter((jnp.dot(conv_out, convolution_output_weight, preferred_...  22 us
    dot_general x6, matrix products, on_device(): jnp.dot(normed, weight, preferred_element_type=jnp.float32)  13.9 us
    all_gather x1, waiting for transfers between devices, on_device(): lax.all_gather(tokens, 'tp', axis=1, tiled=True).astype(jnp.float32)  11.8 us
    dot_general x1, matrix products, on_device(): jnp.dot(attn_out, attention_output_weight, preferred_element_type=jnp.flo...  7.02 us
    add x6, other arithmetic, carry_step(): return (block_decay[..., None] * state + update, state)  6.13 us
    dot_general x1, matrix products, on_device(): jnp.dot(conv_out, convolution_output_weight, preferred_element_type=jnp.f...  6.1 us
    dot_general x1, matrix products, on_device(): jnp.einsum('nchd,nhde->nche', query_g, entering, precision=lax.Precision....  5.72 us
  transfers between devices with their start and end apart: 4, of which 2 were waited for; matrix products, arithmetic and copies ran while one was open for 13% of the time, Pallas kernels for 0%

commit v1 on v0

v1 whole, which is shorter than its diff:
```python
import functools

import jax
import jax.numpy as jnp
from jax import lax
from jax.experimental import pallas as pl
from jax.experimental.pallas import tpu as pltpu
from jax.sharding import PartitionSpec as P

BLOCK = 64
NORM_EPS = 1e-06
GATE_SOFTNESS = 16.0
CHUNK = 256
OUT_CHUNKS = 4
F32, BF16 = jnp.float32, jnp.bfloat16
NT = (((1,), (1,)), ((), ()))
TN = (((0,), (0,)), ((), ()))


def radices(n):
    found = []
    while n > 1:
        r = 4 if n % 4 == 0 else (2 if n % 2 == 0 else n)
        found.append(r)
        n //= r
    return found


def dot32(a, b, dims=(((1,), (0,)), ((), ()))):
    return lax.dot_general(
        a, b, dims, precision=lax.Precision.HIGHEST, preferred_element_type=F32
    )


def dot16(a, b, dims=(((1,), (0,)), ((), ()))):
    return lax.dot_general(a, b, dims, preferred_element_type=F32)


def same_group(shape, row_size, col_size):
    rows = lax.broadcasted_iota(jnp.int32, shape, 0) // row_size
    cols = lax.broadcasted_iota(jnp.int32, shape, 1) // col_size
    return rows == cols


def kernel(n, sizes, *refs):
    rows, feats, heads, dk, dv, cw, widths = sizes
    qk, vw = heads * dk, heads * dv
    (x_ref, gain_ref, wb, wc, wh, taps_ref, wq, wk, wv, wf, wg, bias_ref, extra_ref,
     init_ref, hgain_ref, wco, wao, out_ref,
     wall, wout, nrm, peer, pj, qg_s, kg_s, inner_s, enter_s, excl_s, maskk, maskv,
     prf, halo_s, halo_r, cat, msg, back_s, back_r, wsem, ssem, rsem) = refs
    sp, tp = lax.axis_index("sp"), lax.axis_index("tp")
    levels = radices(n)
    order = (wf, wk, wv, wq, wc, wh, wb, wg)
    loads = []
    at = 0
    offs = []
    for i, (w, width) in enumerate(zip(order, widths)):
        loads.append(pltpu.make_async_copy(w, wall.at[:, at:at + width], wsem.at[i]))
        offs.append(at)
        at += width
    loads.append(pltpu.make_async_copy(wco, wout.at[0:cw, :], wsem.at[8]))
    loads.append(pltpu.make_async_copy(wao, wout.at[cw:cw + vw, :], wsem.at[9]))
    o_f, o_k, o_v, o_q, o_c, o_h, o_b, o_g = offs
    for c in loads[:4]:
        c.start()

    partner = {"tp": 1 - tp}
    nxt = {"sp": lax.rem(sp + 1, n)}
    prv = {"sp": lax.rem(sp + n - 1, n)}
    peers = []
    stride = 1
    for r in levels:
        digit = lax.rem(sp // stride, r)
        base = sp - digit * stride
        peers.append((r, digit, [
            {"sp": base + lax.rem(digit + o, r) * stride} for o in range(1, r)
        ]))
        stride *= r
    everyone = [partner, nxt, prv] + [d for _, _, ds in peers for d in ds]
    barrier = pltpu.get_barrier_semaphore()
    for d in everyone:
        pl.semaphore_signal(barrier, inc=1, device_id=d, device_id_type=pl.DeviceIdType.MESH)
    pl.semaphore_wait(barrier, len(everyone))

    def remote(src, dst, k, device):
        return pltpu.make_async_remote_copy(
            src_ref=src, dst_ref=dst, send_sem=ssem.at[k], recv_sem=rsem.at[k],
            device_id=device, device_id_type=pl.DeviceIdType.MESH,
        )

    swap = remote(x_ref, peer, 0, partner)
    swap.start()
    for c in loads[4:]:
        c.start()

    maskk[...] = jnp.where(same_group(maskk.shape, BLOCK, dk), 1.0, 0.0).astype(BF16)
    maskv[...] = jnp.where(same_group(maskv.shape, BLOCK, dv), 1.0, 0.0).astype(BF16)
    half = feats // 2
    mine = pl.ds(pl.multiple_of(tp * half, half), half)
    theirs = pl.ds(pl.multiple_of((1 - tp) * half, half), half)
    swap.wait()

    def norm_rows(i, carry):
        r = pl.ds(pl.multiple_of(i * 32, 32), 32)
        a, b = x_ref[r, :].astype(F32), peer[r, :].astype(F32)
        power = (
            jnp.sum(a * a, axis=1, keepdims=True) + jnp.sum(b * b, axis=1, keepdims=True)
        ) * (1.0 / feats)
        scale = lax.rsqrt(power + NORM_EPS)
        nrm[r, mine] = (a * scale * gain_ref[:, mine]).astype(BF16)
        nrm[r, theirs] = (b * scale * gain_ref[:, theirs]).astype(BF16)
        return carry

    lax.fori_loop(0, rows // 32, norm_rows, 0)

    def project(first, last):
        def one(i, carry):
            c = pl.ds(pl.multiple_of(i * CHUNK, CHUNK), CHUNK)
            pj[:, c] = dot16(nrm[...], wall[:, c]).astype(BF16)
            return carry

        lax.fori_loop(first // CHUNK, last // CHUNK, one, 0)

    for c in loads[:4]:
        c.wait()
    project(0, o_c)

    n_blocks = rows // BLOCK
    tri_r = lax.broadcasted_iota(jnp.int32, (BLOCK, BLOCK), 0)
    tri_c = lax.broadcasted_iota(jnp.int32, (BLOCK, BLOCK), 1)
    tri = jnp.where(tri_r >= tri_c, 1.0, 0.0)
    spread = jnp.where(same_group((heads, qk), 1, dk), 1.0, 0.0)
    state = jnp.zeros((dv, qk), F32)
    total = jnp.zeros((1, qk), F32)
    for b in range(n_blocks):
        r = slice(b * BLOCK, (b + 1) * BLOCK)
        z = pj[r, o_f:o_f + qk].astype(F32) + bias_ref[...]
        decay = (jnp.minimum(z, 0.0) - jnp.log1p(jnp.exp(-jnp.abs(z)))) * (1.0 / GATE_SOFTNESS)
        decay = decay + dot32(extra_ref[r, :], spread)
        cum = dot32(tri, decay)
        last = cum[BLOCK - 1:BLOCK, :]
        keys = pj[r, o_k:o_k + qk].astype(F32)
        kdec = (keys * jnp.exp(last - cum)).astype(BF16)
        full = dot16(pj[r, o_v:o_v + vw], kdec, TN)
        update = jnp.zeros((dv, qk), F32)
        for h in range(heads):
            s = slice(h * dv, (h + 1) * dv)
            update = update + full[s, :] * maskk[s, :].astype(F32)
        kg_s[r, :] = (keys * jnp.exp(-cum)).astype(BF16)
        qg_s[r, :] = (
            pj[r, o_q:o_q + qk].astype(F32) * dk ** (-0.5) * jnp.exp(cum)
        ).astype(BF16)
        enter_s[b] = state
        excl_s[b] = jnp.broadcast_to(jnp.exp(total), (8, qk))
        state = state * jnp.exp(last) + update
        total = total + last

    pre_s, pre_d = jnp.zeros((dv, qk), F32), jnp.ones((1, qk), F32)
    tot_s, tot_d = state, jnp.exp(total)

    def send_level(lv, tot_s, tot_d):
        r, digit, ds = peers[lv]
        msg[lv, 0, 0:dv, :] = tot_s
        msg[lv, 0, dv:dv + 8, :] = jnp.broadcast_to(tot_d, (8, qk))
        copies = [
            remote(msg.at[lv, 0], msg.at[lv, o], 8 + lv * 4 + o, ds[o - 1]) for o in range(1, r)
        ]
        for c in copies:
            c.start()
        return copies

    def join_level(lv, copies, pre_s, pre_d):
        r, digit, _ = peers[lv]
        for c in copies:
            c.wait()
        low_s, low_d = jnp.zeros((dv, qk), F32), jnp.ones((1, qk), F32)
        all_s, all_d = low_s, low_d
        for j in range(r):
            slot = lax.rem(digit + r - j, r)
            part_s = msg[lv, slot, 0:dv, :]
            part_d = msg[lv, slot, dv:dv + 1, :]
            all_s, all_d = part_d * all_s + part_s, all_d * part_d
            before = j < digit
            low_s = jnp.where(before, all_s, low_s)
            low_d = jnp.where(before, all_d, low_d)
        return all_s, all_d, pre_d * low_s + pre_s, low_d * pre_d

    copies = send_level(0, tot_s, tot_d) if levels else []

    for c in loads[4:8]:
        c.wait()
    project(o_c, o_b)
    for b in range(n_blocks):
        r = slice(b * BLOCK, (b + 1) * BLOCK)
        product = (
            pj[r, o_c:o_c + cw].astype(F32) * pj[r, o_h:o_h + cw].astype(F32)
        ).astype(BF16)
        prf[8 + b * BLOCK:8 + (b + 1) * BLOCK, :] = product.astype(F32)
        if b == n_blocks - 1:
            halo_s[...] = product[BLOCK - 16:, :]
    halo = remote(halo_s, halo_r, 1, nxt)
    halo.start()

    if levels:
        tot_s, tot_d, pre_s, pre_d = join_level(0, copies, pre_s, pre_d)
    if len(levels) > 1:
        copies = send_level(1, tot_s, tot_d)

    project(o_b, o_g + vw)
    causal_r = lax.broadcasted_iota(jnp.int32, (BLOCK, heads * BLOCK), 0)
    causal_c = lax.rem(lax.broadcasted_iota(jnp.int32, (BLOCK, heads * BLOCK), 1), BLOCK)
    causal = causal_r >= causal_c
    for b in range(n_blocks):
        r = slice(b * BLOCK, (b + 1) * BLOCK)
        kst = jnp.concatenate([kg_s[r, :]] * heads, axis=0) * maskk[...]
        scores = jnp.where(causal, dot16(qg_s[r, :], kst, NT), 0.0).astype(BF16)
        vst = jnp.concatenate([pj[r, o_v:o_v + vw]] * heads, axis=0) * maskv[...]
        inner_s[r, :] = dot16(scores, vst)

    halo.wait()
    prf[0:8, :] = jnp.where(sp > 0, halo_r[8:16, :].astype(F32), 0.0)
    taps = taps_ref[...].astype(F32)
    count = taps.shape[0]
    for b in range(n_blocks):
        conv = jnp.zeros((BLOCK, cw), F32)
        for j in range(count):
            start = 8 + b * BLOCK - (count - 1) + j
            conv = conv + taps[j:j + 1, :] * prf[start:start + BLOCK, :]
        r = slice(b * BLOCK, (b + 1) * BLOCK)
        cat[r, 0:cw] = (pj[r, o_b:o_b + cw].astype(F32) * conv).astype(BF16)

    for lv in range(1, len(levels)):
        tot_s, tot_d, pre_s, pre_d = join_level(lv, copies, pre_s, pre_d)
        if lv + 1 < len(levels):
            copies = send_level(lv + 1, tot_s, tot_d)

    eye = jnp.where(
        lax.broadcasted_iota(jnp.int32, (dv, dv), 0)
        == lax.broadcasted_iota(jnp.int32, (dv, dv), 1), 1.0, 0.0)
    incoming = pre_s + pre_d * dot32(eye, init_ref[...], NT)
    repeat = jnp.where(
        lax.broadcasted_iota(jnp.int32, (dv, vw), 0)
        == lax.rem(lax.broadcasted_iota(jnp.int32, (dv, vw), 1), dv), 1.0, 0.0)
    hgain = dot32(jnp.broadcast_to(hgain_ref[...], (8, dv)), repeat)[0:1, :]
    for b in range(n_blocks):
        r = slice(b * BLOCK, (b + 1) * BLOCK)
        entering = (enter_s[b] + excl_s[b, 0:1, :] * incoming).astype(BF16)
        sst = jnp.concatenate([entering] * heads, axis=0) * maskk[...]
        raw = inner_s[r, :] + dot16(qg_s[r, :], sst, NT)
        power = dot16((raw * raw).astype(BF16), maskv[...]) * (1.0 / dv)
        gate = pj[r, o_g:o_g + vw].astype(F32)
        gate = gate / (1.0 + jnp.exp(-gate))
        cat[r, cw:cw + vw] = (raw * lax.rsqrt(power + NORM_EPS) * hgain * gate).astype(BF16)

    for c in loads[8:]:
        c.wait()
    own = rows // 2
    my_rows = pl.ds(pl.multiple_of(tp * own, own), own)
    peer_rows = pl.ds(pl.multiple_of((1 - tp) * own, own), own)
    step = feats // OUT_CHUNKS
    backs = []
    for i in range(OUT_CHUNKS):
        c = slice(i * step, (i + 1) * step)
        back_s[i] = dot16(cat[peer_rows, :], wout[:, c]).astype(BF16)
        backs.append(remote(back_s.at[i], back_r.at[i], 2 + i, partner))
        backs[-1].start()
    for i in range(OUT_CHUNKS):
        c = slice(i * step, (i + 1) * step)
        part = dot16(cat[my_rows, :], wout[:, c])
        backs[i].wait()
        out_ref[:, c] = (part + back_r[i].astype(F32)).astype(BF16)


def on_device(n, tokens, gain, wb, wc, wh, taps, wq, wk, wv, wf, wg, bias, extra, init,
              hgain, wco, wao):
    rows = tokens.shape[0]
    feats = gain.shape[0]
    heads, dk, dv = init.shape
    cw = wb.shape[1]
    qk, vw = heads * dk, heads * dv
    widths = tuple(w.shape[1] for w in (wf, wk, wv, wq, wc, wh, wb, wg))
    sizes = (rows, feats, heads, dk, dv, cw, widths)
    vm, hbm = pl.BlockSpec(memory_space=pltpu.VMEM), pl.BlockSpec(memory_space=pl.ANY)
    n_blocks = rows // BLOCK
    levels = max(len(radices(n)), 1)
    out_rows = rows // 2
    step = feats // OUT_CHUNKS
    n_sems = 8 + 4 * levels
    return pl.pallas_call(
        functools.partial(kernel, n, sizes),
        out_shape=jax.ShapeDtypeStruct((out_rows, feats), BF16),
        in_specs=[vm, vm, hbm, hbm, hbm, vm, hbm, hbm, hbm, hbm, hbm, vm, vm, vm, vm, hbm, hbm],
        out_specs=vm,
        scratch_shapes=[
            pltpu.VMEM((feats, sum(widths)), BF16),
            pltpu.VMEM((cw + vw, feats), BF16),
            pltpu.VMEM((rows, feats), BF16),
            pltpu.VMEM((rows, feats // 2), BF16),
            pltpu.VMEM((rows, sum(widths)), BF16),
            pltpu.VMEM((rows, qk), BF16),
            pltpu.VMEM((rows, qk), BF16),
            pltpu.VMEM((rows, vw), F32),
            pltpu.VMEM((n_blocks, dv, qk), F32),
            pltpu.VMEM((n_blocks, 8, qk), F32),
            pltpu.VMEM((heads * BLOCK, qk), BF16),
            pltpu.VMEM((heads * BLOCK, vw), BF16),
            pltpu.VMEM((rows + 8, cw), F32),
            pltpu.VMEM((16, cw), BF16),
            pltpu.VMEM((16, cw), BF16),
            pltpu.VMEM((rows, cw + vw), BF16),
            pltpu.VMEM((levels, 4, dv + 8, qk), F32),
            pltpu.VMEM((OUT_CHUNKS, out_rows, step), BF16),
            pltpu.VMEM((OUT_CHUNKS, out_rows, step), BF16),
            pltpu.SemaphoreType.DMA((10,)),
            pltpu.SemaphoreType.DMA((n_sems,)),
            pltpu.SemaphoreType.DMA((n_sems,)),
        ],
        compiler_params=pltpu.CompilerParams(
            collective_id=0, has_side_effects=True, vmem_limit_bytes=60 * 2**20
        ),
        name="mixer",
    )(
        tokens, gain.reshape(1, feats), wb, wc, wh, taps, wq, wk, wv, wf, wg,
        bias.reshape(1, qk), extra, init.reshape(qk, dv), hgain.reshape(1, dv), wco, wao,
    )


def solution(mesh):
    placed = (
        P("sp", "tp"), P(), P(None, "tp"), P(None, "tp"), P(None, "tp"), P(None, "tp"),
        P(None, "tp"), P(None, "tp"), P(None, "tp"), P(None, "tp"), P(None, "tp"),
        P("tp"), P("sp", "tp"), P("tp", None, None), P(), P("tp", None), P("tp", None),
    )
    return jax.shard_map(
        functools.partial(on_device, mesh.shape["sp"]), mesh=mesh, in_specs=placed,
        out_specs=P(("sp", "tp"), None), check_vma=False,
    )
```

time: 177 us -> 38.7 us (0.22)
  matrix products: 42 us -> 0 us
  blocking collectives: 39.2 us -> 0 us
  Pallas kernels: 0 us -> 34.8 us
  waiting for transfers between devices: 34.5 us -> 0 us
  other arithmetic: 21.3 us -> 0 us
  local copies, waits for them, and re-layouts: 21.5 us -> 3.6 us
  between operations: 13.4 us -> 0.01 us
  starting transfers between devices: 3.88 us -> 0 us
    dot_general x12 -> x0, matrix products: 42 us -> none  [the longest x6 13.9 us: on_device(): jnp.dot(normed, weight, preferred_element_type=jnp.float32)]
    all_gather x1 -> x0, blocking collectives: 39.2 us -> none  [prefix(): gathered = jax.tree.map(lambda a: lax.all_gather(a, axis), part)]
    pallas_call x0 -> x1, Pallas kernels: none -> 34.8 us  [on_device(): pl.pallas_call(functools.partial(kernel, n, sizes), out_shape=jax.ShapeDt...]
    reduce_scatter x1 -> x0, waiting for transfers between devices: 22 us -> none  [on_device(): lax.psum_scatter((jnp.dot(conv_out, convolution_output_weight, preferred_...]
    all_gather x2 -> x0, waiting for transfers between devices: 11.8 us -> none  [the longest x1 11.8 us: on_device(): lax.all_gather(tokens, 'tp', axis=1, tiled=True).astype(jnp.float32)]
    reshape x5 -> x0, local copies, waits for them, and re-layouts: 7.32 us -> none  [the longest x1 2.65 us: on_device(): raw = (inner + outer).reshape(number_of_rows, number_of_heads, value_dim)]
    add x8 -> x0, other arithmetic: 7.29 us -> none  [the longest x6 6.13 us: carry_step(): return (block_decay[..., None] * state + update, state)]
    add x3 -> x0, local copies, waits for them, and re-layouts: 6.7 us -> none  [the longest x2 3.66 us: on_device(): logarithm_decay.reshape(number_of_rows, number_of_heads, key_channel_count)]
  transfers between devices with their start and end apart: 4 -> 0, of which waited for: 2 -> 0; matrix products, arithmetic and copies ran while one was open for 13% -> 0% of each run, Pallas kernels for 0% -> 0%
where the time goes in v1:
time: 38.7 us; the launch traced here: 38.4 us
  Pallas kernels  34.8 us (90%)
  local copies, waits for them, and re-layouts  3.6 us (9%)
    pallas_call x1, Pallas kernels, on_device(): pl.pallas_call(functools.partial(kernel, n, sizes), out_shape=jax.ShapeDt...  34.8 us
    unnamed x2, local copies, waits for them, and re-layouts  3.6 us

profile of v1, /device:TPU:0, one launch (start us, length us, event | category | flops | bytes accessed | tf_op | source)
XLA Modules:
  0.0 38.4 jit_solution(12890903020869515261)
XLA Ops:
  0.0 1.5 %copy.18.refs_12_ = f32[384,8]{1,0:T(8,128)} copy(f32[384,8]{0,1:T(8,128)} %param.29) | data formatting | bytes 24576 | tf_op args[12]
  1.5 34.8 %mixer.1 = bf16[192,2048]{1,0:T(8,128)(2,1)} custom-call(bf16[384,1024]{1,0:T(8,128)(2,1)} %refs_0_.1, f32[1,2048]{1,0:T(1,128)} %bitcast.5, bf16[2048,512]{1,0:T(8,128)(2,1)} %refs_2_.1, bf16[2048,512]{1,0:T(8,128)(2,1)} %refs_3_.1, bf16[2048,512]{1,0:T(8,128)(2,1)} %refs_4_.1, bf16[3,512]{1,0:T(4,128)(2,1)} %refs_5_.1, bf16[2048,256]{1,0:T(8,128)(2,1)} %refs_6_.1, ...), custom_call_target="tpu_custom_call" | custom-call | tf_op jit(solution)/shard_map/mixer/pallas_call | solution.py:290
  36.3 2.1 %copy.20 = bf16[192,2048]{1,0:T(8,128)(2,1)} copy(bf16[192,2048]{1,0:T(8,128)(2,1)} %mixer.1) | data formatting | bytes 1572864

commit v2 on v1

--- a/solution.py
+++ b/solution.py
@@ -47,22 +47,27 @@
     qk, vw = heads * dk, heads * dv
     (x_ref, gain_ref, wb, wc, wh, taps_ref, wq, wk, wv, wf, wg, bias_ref, extra_ref,
      init_ref, hgain_ref, wco, wao, out_ref,
-     wall, wout, nrm, peer, pj, qg_s, kg_s, inner_s, enter_s, excl_s, maskk, maskv,
+     wall, wout, ya, yb, peer, acc, scale_s, ext_s, oacc, pj, qg_s, kg_s, inner_s, enter_s, excl_s, maskk, maskv,
      prf, halo_s, halo_r, cat, msg, back_s, back_r, wsem, ssem, rsem) = refs
     sp, tp = lax.axis_index("sp"), lax.axis_index("tp")
     levels = radices(n)
     order = (wf, wk, wv, wq, wc, wh, wb, wg)
-    loads = []
+    half = feats // 2
+    mine = pl.ds(pl.multiple_of(tp * half, half), half)
+    theirs = pl.ds(pl.multiple_of((1 - tp) * half, half), half)
+    first, second, offs = [], [], []
     at = 0
-    offs = []
     for i, (w, width) in enumerate(zip(order, widths)):
-        loads.append(pltpu.make_async_copy(w, wall.at[:, at:at + width], wsem.at[i]))
+        for j, (part, found) in enumerate(((mine, first), (theirs, second))):
+            found.append(pltpu.make_async_copy(
+                w.at[part, :], wall.at[part, at:at + width], wsem.at[8 * j + i]))
         offs.append(at)
         at += width
-    loads.append(pltpu.make_async_copy(wco, wout.at[0:cw, :], wsem.at[8]))
-    loads.append(pltpu.make_async_copy(wao, wout.at[cw:cw + vw, :], wsem.at[9]))
+    end = at
+    load_co = pltpu.make_async_copy(wco, wout.at[0:cw, :], wsem.at[16])
+    load_ao = pltpu.make_async_copy(wao, wout.at[cw:cw + vw, :], wsem.at[17])
     o_f, o_k, o_v, o_q, o_c, o_h, o_b, o_g = offs
-    for c in loads[:4]:
+    for c in first + second + [load_co, load_ao]:
         c.start()
 
     partner = {"tp": 1 - tp}
@@ -77,11 +82,10 @@
             {"sp": base + lax.rem(digit + o, r) * stride} for o in range(1, r)
         ]))
         stride *= r
-    everyone = [partner, nxt, prv] + [d for _, _, ds in peers for d in ds]
+    everyone = [partner] + [d for _, _, ds in peers for d in ds]
     barrier = pltpu.get_barrier_semaphore()
     for d in everyone:
         pl.semaphore_signal(barrier, inc=1, device_id=d, device_id_type=pl.DeviceIdType.MESH)
-    pl.semaphore_wait(barrier, len(everyone))
 
     def remote(src, dst, k, device):
         return pltpu.make_async_remote_copy(
@@ -89,40 +93,66 @@
             device_id=device, device_id_type=pl.DeviceIdType.MESH,
         )
 
+    @pl.when(sp < n - 1)
+    def _():
+        pl.semaphore_signal(barrier, inc=1, device_id=nxt, device_id_type=pl.DeviceIdType.MESH)
+
+    @pl.when(sp > 0)
+    def _():
+        pl.semaphore_signal(barrier, inc=1, device_id=prv, device_id_type=pl.DeviceIdType.MESH)
+
     swap = remote(x_ref, peer, 0, partner)
+
+    def own_rows(i, carry):
+        r = pl.ds(pl.multiple_of(i * 32, 32), 32)
+        a = x_ref[r, :].astype(F32)
+        ya[r, :] = (a * gain_ref[:, mine]).astype(BF16)
+        scale_s[r, :] = jnp.broadcast_to(
+            jnp.sum(a * a, axis=1, keepdims=True), (32, CHUNK))
+        return carry
+
+    def peer_rows_in(i, carry):
+        r = pl.ds(pl.multiple_of(i * 32, 32), 32)
+        b = peer[r, :].astype(F32)
+        yb[r, :] = (b * gain_ref[:, theirs]).astype(BF16)
+        power = (scale_s[r, :] + jnp.sum(b * b, axis=1, keepdims=True)) * (1.0 / feats)
+        scale_s[r, :] = lax.rsqrt(power + NORM_EPS)
+        return carry
+
+    def project_own(lo, hi):
+        def one(i, carry):
+            c = pl.ds(pl.multiple_of(i * CHUNK, CHUNK), CHUNK)
+            acc[:, c] = dot16(ya[...], wall[mine, c])
+            return carry
+
+        lax.fori_loop(lo // CHUNK, hi // CHUNK, one, 0, unroll=True)
+
+    def project(lo, hi):
+        def one(i, carry):
+            c = pl.ds(pl.multiple_of(i * CHUNK, CHUNK), CHUNK)
+            whole = acc[:, c] + dot16(yb[...], wall[theirs, c])
+            pj[:, c] = (whole * scale_s[...]).astype(BF16)
+            return carry
+
+        lax.fori_loop(lo // CHUNK, hi // CHUNK, one, 0, unroll=True)
+
+    lax.fori_loop(0, rows // 32, own_rows, 0)
+    for c in first[:4]:
+        c.wait()
+    project_own(0, o_c)
+    ends = jnp.where(sp > 0, 1, 0) + jnp.where(sp < n - 1, 1, 0)
+    pl.semaphore_wait(barrier, len(everyone) + ends)
     swap.start()
-    for c in loads[4:]:
-        c.start()
-
+    for c in first[4:]:
+        c.wait()
+    project_own(o_c, end)
     maskk[...] = jnp.where(same_group(maskk.shape, BLOCK, dk), 1.0, 0.0).astype(BF16)
     maskv[...] = jnp.where(same_group(maskv.shape, BLOCK, dv), 1.0, 0.0).astype(BF16)
-    half = feats // 2
-    mine = pl.ds(pl.multiple_of(tp * half, half), half)
-    theirs = pl.ds(pl.multiple_of((1 - tp) * half, half), half)
+    spread = jnp.where(same_group((heads, qk), 1, dk), 1.0, 0.0)
+    ext_s[...] = dot32(extra_ref[...], spread, TN)
     swap.wait()
-
-    def norm_rows(i, carry):
-        r = pl.ds(pl.multiple_of(i * 32, 32), 32)
-        a, b = x_ref[r, :].astype(F32), peer[r, :].astype(F32)
-        power = (
-            jnp.sum(a * a, axis=1, keepdims=True) + jnp.sum(b * b, axis=1, keepdims=True)
-        ) * (1.0 / feats)
-        scale = lax.rsqrt(power + NORM_EPS)
-        nrm[r, mine] = (a * scale * gain_ref[:, mine]).astype(BF16)
-        nrm[r, theirs] = (b * scale * gain_ref[:, theirs]).astype(BF16)
-        return carry
-
-    lax.fori_loop(0, rows // 32, norm_rows, 0)
-
-    def project(first, last):
-        def one(i, carry):
-            c = pl.ds(pl.multiple_of(i * CHUNK, CHUNK), CHUNK)
-            pj[:, c] = dot16(nrm[...], wall[:, c]).astype(BF16)
-            return carry
-
-        lax.fori_loop(first // CHUNK, last // CHUNK, one, 0)
-
-    for c in loads[:4]:
+    lax.fori_loop(0, rows // 32, peer_rows_in, 0)
+    for c in second[:4]:
         c.wait()
     project(0, o_c)
 
@@ -130,14 +160,13 @@
     tri_r = lax.broadcasted_iota(jnp.int32, (BLOCK, BLOCK), 0)
     tri_c = lax.broadcasted_iota(jnp.int32, (BLOCK, BLOCK), 1)
     tri = jnp.where(tri_r >= tri_c, 1.0, 0.0)
-    spread = jnp.where(same_group((heads, qk), 1, dk), 1.0, 0.0)
     state = jnp.zeros((dv, qk), F32)
     total = jnp.zeros((1, qk), F32)
     for b in range(n_blocks):
         r = slice(b * BLOCK, (b + 1) * BLOCK)
         z = pj[r, o_f:o_f + qk].astype(F32) + bias_ref[...]
         decay = (jnp.minimum(z, 0.0) - jnp.log1p(jnp.exp(-jnp.abs(z)))) * (1.0 / GATE_SOFTNESS)
-        decay = decay + dot32(extra_ref[r, :], spread)
+        decay = decay + ext_s[r, :]
         cum = dot32(tri, decay)
         last = cum[BLOCK - 1:BLOCK, :]
         keys = pj[r, o_k:o_k + qk].astype(F32)
@@ -161,8 +190,11 @@
 
     def send_level(lv, tot_s, tot_d):
         r, digit, ds = peers[lv]
-        msg[lv, 0, 0:dv, :] = tot_s
-        msg[lv, 0, dv:dv + 8, :] = jnp.broadcast_to(tot_d, (8, qk))
+        high = tot_d.astype(BF16).astype(F32)
+        msg[lv, 0, 0:dv, :] = tot_s.astype(BF16)
+        msg[lv, 0, dv:dv + 16, :] = jnp.concatenate([
+            jnp.broadcast_to(high, (8, qk)), jnp.broadcast_to(tot_d - high, (8, qk))
+        ], axis=0).astype(BF16)
         copies = [
             remote(msg.at[lv, 0], msg.at[lv, o], 8 + lv * 4 + o, ds[o - 1]) for o in range(1, r)
         ]
@@ -178,8 +210,9 @@
         all_s, all_d = low_s, low_d
         for j in range(r):
             slot = lax.rem(digit + r - j, r)
-            part_s = msg[lv, slot, 0:dv, :]
-            part_d = msg[lv, slot, dv:dv + 1, :]
+            part_s = msg[lv, slot, 0:dv, :].astype(F32)
+            pair = msg[lv, slot, dv:dv + 16, :].astype(F32)
+            part_d = pair[0:1, :] + pair[8:9, :]
             all_s, all_d = part_d * all_s + part_s, all_d * part_d
             before = j < digit
             low_s = jnp.where(before, all_s, low_s)
@@ -188,7 +221,7 @@
 
     copies = send_level(0, tot_s, tot_d) if levels else []
 
-    for c in loads[4:8]:
+    for c in second[4:]:
         c.wait()
     project(o_c, o_b)
     for b in range(n_blocks):
@@ -200,14 +233,18 @@
         if b == n_blocks - 1:
             halo_s[...] = product[BLOCK - 16:, :]
     halo = remote(halo_s, halo_r, 1, nxt)
-    halo.start()
+
+    @pl.when(sp < n - 1)
+    def _():
+        halo.start()
+
+    project(o_b, end)
 
     if levels:
         tot_s, tot_d, pre_s, pre_d = join_level(0, copies, pre_s, pre_d)
     if len(levels) > 1:
         copies = send_level(1, tot_s, tot_d)
 
-    project(o_b, o_g + vw)
     causal_r = lax.broadcasted_iota(jnp.int32, (BLOCK, heads * BLOCK), 0)
     causal_c = lax.rem(lax.broadcasted_iota(jnp.int32, (BLOCK, heads * BLOCK), 1), BLOCK)
     causal = causal_r >= causal_c
@@ -218,8 +255,19 @@
         vst = jnp.concatenate([pj[r, o_v:o_v + vw]] * heads, axis=0) * maskv[...]
         inner_s[r, :] = dot16(scores, vst)
 
-    halo.wait()
-    prf[0:8, :] = jnp.where(sp > 0, halo_r[8:16, :].astype(F32), 0.0)
+    @pl.when(sp < n - 1)
+    def _():
+        halo.wait_send()
+
+    @pl.when(sp > 0)
+    def _():
+        halo.wait_recv()
+        prf[0:8, :] = halo_r[8:16, :].astype(F32)
+
+    @pl.when(sp == 0)
+    def _():
+        prf[0:8, :] = jnp.zeros((8, cw), F32)
+
     taps = taps_ref[...].astype(F32)
     count = taps.shape[0]
     for b in range(n_blocks):
@@ -229,6 +277,12 @@
             conv = conv + taps[j:j + 1, :] * prf[start:start + BLOCK, :]
         r = slice(b * BLOCK, (b + 1) * BLOCK)
         cat[r, 0:cw] = (pj[r, o_b:o_b + cw].astype(F32) * conv).astype(BF16)
+
+    step = feats // OUT_CHUNKS
+    load_co.wait()
+    for i in range(OUT_CHUNKS):
+        c = slice(i * step, (i + 1) * step)
+        oacc[:, c] = dot16(cat[:, 0:cw], wout[0:cw, c])
 
     for lv in range(1, len(levels)):
         tot_s, tot_d, pre_s, pre_d = join_level(lv, copies, pre_s, pre_d)
@@ -253,21 +307,21 @@
         gate = gate / (1.0 + jnp.exp(-gate))
         cat[r, cw:cw + vw] = (raw * lax.rsqrt(power + NORM_EPS) * hgain * gate).astype(BF16)
 
-    for c in loads[8:]:
-        c.wait()
+    load_ao.wait()
     own = rows // 2
     my_rows = pl.ds(pl.multiple_of(tp * own, own), own)
     peer_rows = pl.ds(pl.multiple_of((1 - tp) * own, own), own)
-    step = feats // OUT_CHUNKS
     backs = []
     for i in range(OUT_CHUNKS):
         c = slice(i * step, (i + 1) * step)
-        back_s[i] = dot16(cat[peer_rows, :], wout[:, c]).astype(BF16)
+        back_s[i] = (
+            oacc[peer_rows, c] + dot16(cat[peer_rows, cw:cw + vw], wout[cw:cw + vw, c])
+        ).astype(BF16)
         backs.append(remote(back_s.at[i], back_r.at[i], 2 + i, partner))
         backs[-1].start()
     for i in range(OUT_CHUNKS):
         c = slice(i * step, (i + 1) * step)
-        part = dot16(cat[my_rows, :], wout[:, c])
+        part = oacc[my_rows, c] + dot16(cat[my_rows, cw:cw + vw], wout[cw:cw + vw, c])
         backs[i].wait()
         out_ref[:, c] = (part + back_r[i].astype(F32)).astype(BF16)
 
@@ -295,8 +349,13 @@
         scratch_shapes=[
             pltpu.VMEM((feats, sum(widths)), BF16),
             pltpu.VMEM((cw + vw, feats), BF16),
-            pltpu.VMEM((rows, feats), BF16),
             pltpu.VMEM((rows, feats // 2), BF16),
+            pltpu.VMEM((rows, feats // 2), BF16),
+            pltpu.VMEM((rows, feats // 2), BF16),
+            pltpu.VMEM((rows, sum(widths)), F32),
+            pltpu.VMEM((rows, CHUNK), F32),
+            pltpu.VMEM((rows, qk), F32),
+            pltpu.VMEM((rows, feats), F32),
             pltpu.VMEM((rows, sum(widths)), BF16),
             pltpu.VMEM((rows, qk), BF16),
             pltpu.VMEM((rows, qk), BF16),
@@ -309,10 +368,10 @@
             pltpu.VMEM((16, cw), BF16),
             pltpu.VMEM((16, cw), BF16),
             pltpu.VMEM((rows, cw + vw), BF16),
-            pltpu.VMEM((levels, 4, dv + 8, qk), F32),
+            pltpu.VMEM((levels, 4, dv + 16, qk), BF16),
             pltpu.VMEM((OUT_CHUNKS, out_rows, step), BF16),
             pltpu.VMEM((OUT_CHUNKS, out_rows, step), BF16),
-            pltpu.SemaphoreType.DMA((10,)),
+            pltpu.SemaphoreType.DMA((18,)),
             pltpu.SemaphoreType.DMA((n_sems,)),
             pltpu.SemaphoreType.DMA((n_sems,)),
         ],
@@ -322,7 +381,7 @@
         name="mixer",
     )(
         tokens, gain.reshape(1, feats), wb, wc, wh, taps, wq, wk, wv, wf, wg,
-        bias.reshape(1, qk), extra, init.reshape(qk, dv), hgain.reshape(1, dv), wco, wao,
+        bias.reshape(1, qk), extra.T, init.reshape(qk, dv), hgain.reshape(1, dv), wco, wao,
     )
 
 

time: 38.7 us -> 30.2 us (0.78)
  Pallas kernels: 34.8 us -> 27.9 us
  local copies, waits for them, and re-layouts: 3.6 us -> 2.09 us
    pallas_call x1, Pallas kernels: 34.8 us -> 27.9 us  [on_device(): pl.pallas_call(functools.partial(kernel, n, sizes), out_shape=jax.ShapeDt...]
    unnamed x2 -> x1, local copies, waits for them, and re-layouts: 3.6 us -> 2.09 us
where the time goes in v2:
time: 30.2 us; the launch traced here: 30 us
  Pallas kernels  27.9 us (92%)
  local copies, waits for them, and re-layouts  2.09 us (7%)
    pallas_call x1, Pallas kernels, on_device(): pl.pallas_call(functools.partial(kernel, n, sizes), out_shape=jax.ShapeDt...  27.9 us
    unnamed x1, local copies, waits for them, and re-layouts  2.09 us

profile of v2, /device:TPU:0, one launch (start us, length us, event | category | flops | bytes accessed | tf_op | source)
XLA Modules:
  0.0 30.0 jit_solution(5493166535226847336)
XLA Ops:
  0.0 27.9 %mixer.1 = bf16[192,2048]{1,0:T(8,128)(2,1)} custom-call(bf16[384,1024]{1,0:T(8,128)(2,1)} %refs_0_.1, f32[1,2048]{1,0:T(1,128)} %bitcast.7, bf16[2048,512]{1,0:T(8,128)(2,1)} %refs_2_.1, bf16[2048,512]{1,0:T(8,128)(2,1)} %refs_3_.1, bf16[2048,512]{1,0:T(8,128)(2,1)} %refs_4_.1, bf16[3,512]{1,0:T(4,128)(2,1)} %refs_5_.1, bf16[2048,256]{1,0:T(8,128)(2,1)} %refs_6_.1, ...), custom_call_target="tpu_custom_call" | custom-call | tf_op jit(solution)/shard_map/mixer/pallas_call | solution.py:344
  27.9 2.1 %copy.19 = bf16[192,2048]{1,0:T(8,128)(2,1)} copy(bf16[192,2048]{1,0:T(8,128)(2,1)} %mixer.1) | data formatting | bytes 1572864
